TPU v7x, 32 devices: a whole 2x2x4 slice. The times are simulated.
32 devices in a mesh: grp: 2 (over y), fs: 4 (over z), tp: 4 (over x, core).
Axes of the slice: x: 2, y: 2, z: 4, core: 2. Of those that a mesh axis runs over, the one named last changes fastest.
Arguments:
- tokens: bfloat16 [4096, 2048], P(('grp', 'fs')), parts along dimension 0, may hold values from -6 to 6
- norm_gain: float32 [2, 2048], replicated, may hold values from 0.1 to 1.9
- norm_shift: float32 [2, 2048], replicated, may hold values from -3 to 3
- gate_first: bfloat16 [2048, 3072], P('fs', 'tp'), may hold values from -0.125 to 0.125
- up_first: bfloat16 [2048, 3072], P('fs', 'tp'), may hold values from -0.125 to 0.125
- down_first: bfloat16 [3072, 2048], P('tp', 'fs'), may hold values from -0.21875 to 0.21875
- gate_second: bfloat16 [2048, 3072], P('fs', 'tp'), may hold values from -0.125 to 0.125
- up_second: bfloat16 [2048, 3072], P('fs', 'tp'), may hold values from -0.125 to 0.125
- down_second: bfloat16 [3072, 2048], P('tp', 'fs'), may hold values from -0.21875 to 0.21875
Outputs:
- encoded: bfloat16 [4096, 2048], P(('grp', 'fs')), parts along dimension 0
There are 2 independent parts, one for each index of `grp`. A program takes and returns all parts, laid end to end along the dimension named above; an argument that names none is the same for every part. Nothing has to cross between parts.
All inputs are finite; a program needn't handle non-finite values.
Results may differ from a plain program's by a relative error of at most 0.012.
Values may be sent and summed in bfloat16 or wider, within the bound.
A program may use at most 64 MiB of HBM per device.

v0:
```python
import jax
import jax.numpy as jnp
from jax import lax
from jax.sharding import PartitionSpec as P


def post_norm(values, gain, shift):
    mean = jnp.mean(values, axis=-1, keepdims=True)
    spread = jnp.mean(jnp.square(values - mean), axis=-1, keepdims=True)
    normed = (values - mean) * lax.rsqrt(spread + 1e-05)
    return (normed * gain + shift).astype(jnp.bfloat16)


def rounded_term(stream_rows, down_full):
    return jnp.dot(stream_rows, down_full, preferred_element_type=jnp.float32).astype(jnp.bfloat16)


def half_step(stream, gate_w, up_w, down_w, gain, shift):
    width = gate_w.shape[1]
    joined = jnp.concatenate(
        (
            lax.all_gather(gate_w, "fs", axis=0, tiled=True),
            lax.all_gather(up_w, "fs", axis=0, tiled=True),
        ),
        axis=1,
    )
    both = jnp.dot(stream, joined, preferred_element_type=jnp.float32)
    gate = both[:, :width]
    up = both[:, width:]
    hidden = (jax.nn.silu(gate) * up).astype(jnp.bfloat16)
    scale = 2.0**0.25
    down_full = lax.all_gather(down_w, "fs", axis=1, tiled=True)
    partial_value = rounded_term(hidden, down_full)
    branch = lax.psum(partial_value, "tp").astype(jnp.float32).astype(jnp.bfloat16)
    return post_norm(
        scale * stream.astype(jnp.float32) + 0.5 * branch.astype(jnp.float32), gain, shift
    )


def local(
    tokens,
    norm_gain,
    norm_shift,
    gate_first,
    up_first,
    down_first,
    gate_second,
    up_second,
    down_second,
):
    middle = half_step(tokens, gate_first, up_first, down_first, norm_gain[0], norm_shift[0])
    return half_step(middle, gate_second, up_second, down_second, norm_gain[1], norm_shift[1])


def solution(mesh):
    placed = (
        P(("grp", "fs"), None),
        P(),
        P(),
        P("fs", "tp"),
        P("fs", "tp"),
        P("tp", "fs"),
        P("fs", "tp"),
        P("fs", "tp"),
        P("tp", "fs"),
    )
    return jax.shard_map(
        local, mesh=mesh, in_specs=placed, out_specs=P(("grp", "fs"), None), check_vma=False
    )
```

profile of v0, /device:TPU:0, one launch (start us, length us, event | category | flops | bytes accessed | tf_op | source)
XLA Modules:
  0.0 519.6 jit_solution(14808185520538437367)
XLA Ops:
  6.5 0.0 all-gather.7.cloned.1.call-start
  6.5 0.7 all-gather.7.cloned.1.call-update
  7.3 0.0 all-gather.9.cloned.1.call-start
  7.3 0.7 all-gather.9.cloned.1.call-update
  8.0 0.0 all-gather.11.cloned.1.call-start
  8.1 0.7 all-gather.11.cloned.1.call-update
  8.7 0.0 all-reduce.3.cloned.1.call-start
  8.8 66.3 %all-gather.7.cloned.1.call-done = bf16[2048,768]{1,0:T(8,128)(2,1)} async-done(((bf16[512,768]{1,0:T(8,128)(2,1)}), bf16[2048,768]{1,0:T(8,128)(2,1)}) %all-gather.7.cloned.1.call-update) | async-done | bytes 3145744 | tf_op jit(solution)/shard_map/all_gather | solution.py:22
  75.1 63.7 %all-gather.9.cloned.1.call-done = bf16[2048,768]{1,0:T(8,128)(2,1)} async-done(((bf16[512,768]{1,0:T(8,128)(2,1)}), bf16[2048,768]{1,0:T(8,128)(2,1)}) %all-gather.9.cloned.1.call-update) | async-done | bytes 3145744 | tf_op jit(solution)/shard_map/all_gather | solution.py:23
  138.8 6.9 %fusion.8 = f32[512,1536]{0,1:T(8,128)S(1)} fusion(bf16[512,2048]{1,0:T(8,128)(2,1)} %param.9, bf16[2048,768]{1,0:T(8,128)(2,1)} %all-gather.9.cloned.1.call-done, bf16[2048,768]{1,0:T(8,128)(2,1)} %all-gather.7.cloned.1.call-done), kind=kOutput, calls=%fused_computation.14 | convolution fusion | flops 3233808384 | bytes 11534336 | tf_op jit(solution)/shard_map/dot_general | solution.py:27
  145.7 56.7 %all-gather.11.cloned.1.call-done = bf16[768,2048]{1,0:T(8,128)(2,1)} async-done(((bf16[768,512]{1,0:T(8,128)(2,1)}), bf16[768,2048]{1,0:T(8,128)(2,1)}) %all-gather.11.cloned.1.call-update) | async-done | bytes 3145744 | tf_op jit(solution)/shard_map/all_gather | solution.py:32
  202.5 5.1 convolution_convert_fusion.1
  207.6 0.0 copy-start.4
  207.6 0.0 copy-start.5
  207.6 0.0 copy-start
  207.6 0.0 all-reduce.3.cloned.1.call-update
  207.6 0.0 all-gather.13.cloned.1.call-start
  207.7 0.5 all-gather.13.cloned.1.call-update
  208.2 0.0 all-gather.15.cloned.1.call-start
  208.3 0.5 all-gather.15.cloned.1.call-update
  208.8 0.0 all-gather.17.cloned.1.call-start
  208.8 0.7 all-gather.17.cloned.1.call-update
  209.5 0.2 all-reduce.5.cloned.1.call-start
  209.8 0.0 copy-done.4
  209.8 0.0 copy-done.5
  209.8 48.0 %all-reduce.3.cloned.1.call-done = bf16[512,2048]{1,0:T(8,128)(2,1)} async-done(((bf16[512,2048]{1,0:T(8,128)(2,1)}), bf16[512,2048]{1,0:T(8,128)(2,1)}) %all-reduce.3.cloned.1.call-update) | async-done | bytes 2097168 | tf_op jit(solution)/shard_map/psum | solution.py:34
  257.8 0.0 copy-done
  257.8 0.0 copy-start.2
  257.8 2.6 fusion.11
  260.4 0.0 copy-start.1
  260.4 0.0 copy-done.2
  260.5 1.2 multiply_reduce_fusion.1
  261.6 0.4 copy-done.1
  262.0 1.3 add_convert_fusion.1
  263.4 59.4 %all-gather.13.cloned.1.call-done = bf16[2048,768]{1,0:T(8,128)(2,1)} async-done(((bf16[512,768]{1,0:T(8,128)(2,1)}), bf16[2048,768]{1,0:T(8,128)(2,1)}) %all-gather.13.cloned.1.call-update) | async-done | bytes 3145744 | tf_op jit(solution)/shard_map/all_gather | solution.py:22
  322.8 63.5 %all-gather.15.cloned.1.call-done = bf16[2048,768]{1,0:T(8,128)(2,1)} async-done(((bf16[512,768]{1,0:T(8,128)(2,1)}), bf16[2048,768]{1,0:T(8,128)(2,1)}) %all-gather.15.cloned.1.call-update) | async-done | bytes 3145744 | tf_op jit(solution)/shard_map/all_gather | solution.py:23
  386.3 8.0 %fusion.4 = f32[512,1536]{0,1:T(8,128)} fusion(bf16[512,2048]{1,0:T(8,128)(2,1)S(1)} %add_convert_fusion.1, bf16[2048,768]{1,0:T(8,128)(2,1)} %all-gather.15.cloned.1.call-done, bf16[2048,768]{1,0:T(8,128)(2,1)} %all-gather.13.cloned.1.call-done), kind=kOutput, calls=%fused_computation.4 | convolution fusion | flops 3233808384 | bytes 11534336 | tf_op jit(solution)/shard_map/dot_general | solution.py:27
  394.3 55.7 %all-gather.17.cloned.1.call-done = bf16[768,2048]{1,0:T(8,128)(2,1)} async-done(((bf16[768,512]{1,0:T(8,128)(2,1)}), bf16[768,2048]{1,0:T(8,128)(2,1)}) %all-gather.17.cloned.1.call-update) | async-done | bytes 3145744 | tf_op jit(solution)/shard_map/all_gather | solution.py:32
  450.0 6.1 %convolution_convert_fusion = bf16[512,2048]{1,0:T(8,128)(2,1)} fusion(bf16[768,2048]{1,0:T(8,128)(2,1)} %all-gather.17.cloned.1.call-done, f32[512,1536]{0,1:T(8,128)} %fusion.4), kind=kOutput, calls=%fused_computation.15 | convolution fusion | flops 1614020608 | bytes 8388608 | tf_op jit(solution)/shard_map/dot_general | solution.py:15
  456.1 0.0 all-reduce.5.cloned.1.call-update
  456.1 50.2 %all-reduce.5.cloned.1.call-done = bf16[512,2048]{1,0:T(8,128)(2,1)} async-done(((bf16[512,2048]{1,0:T(8,128)(2,1)}), bf16[512,2048]{1,0:T(8,128)(2,1)}) %all-reduce.5.cloned.1.call-update) | async-done | bytes 2097168 | tf_op jit(solution)/shard_map/psum | solution.py:34
  506.3 0.0 copy-start.3
  506.3 2.6 fusion.12
  508.9 0.0 copy-done.3
  508.9 1.2 multiply_reduce_fusion
  510.1 2.6 add_convert_fusion
  (6 shorter events, 0.1 us)
Async XLA Ops:
  6.5 68.6 %all-gather.7.cloned.1.call-start = ((), (), s32[]{:S(2)}) async-start(), calls=%async_computation | async-start | bytes 3932160 | tf_op jit(solution)/shard_map/all_gather | solution.py:22
  7.3 131.5 %all-gather.9.cloned.1.call-start = ((), (), s32[]{:S(2)}) async-start(), calls=%async_computation.1 | async-start | bytes 3932160 | tf_op jit(solution)/shard_map/all_gather | solution.py:23
  8.0 194.5 %all-gather.11.cloned.1.call-start = ((), (), s32[]{:S(2)}) async-start(), calls=%async_computation.2 | async-start | bytes 3932160 | tf_op jit(solution)/shard_map/all_gather | solution.py:32
  8.7 249.1 %all-reduce.3.cloned.1.call-start = ((), (), s32[]{:S(2)}) async-start(), calls=%async_computation.3 | async-start | bytes 4194304 | tf_op jit(solution)/shard_map/psum | solution.py:34
  207.6 2.2 copy-start.4
  207.6 2.2 copy-start.5
  207.6 50.2 %copy-start = (bf16[512,2048]{1,0:T(8,128)(2,1)S(1)}, bf16[512,2048]{1,0:T(8,128)(2,1)}, u32[]{:S(2)}) copy-start(bf16[512,2048]{1,0:T(8,128)(2,1)} %param.9) | copy-start | bytes 6291460
  207.6 115.1 %all-gather.13.cloned.1.call-start = ((), (), s32[]{:S(2)}) async-start(), calls=%async_computation.4 | async-start | bytes 3932160 | tf_op jit(solution)/shard_map/all_gather | solution.py:22
  208.2 178.1 %all-gather.15.cloned.1.call-start = ((), (), s32[]{:S(2)}) async-start(), calls=%async_computation.5 | async-start | bytes 3932160 | tf_op jit(solution)/shard_map/all_gather | solution.py:23
  208.8 241.2 %all-gather.17.cloned.1.call-start = ((), (), s32[]{:S(2)}) async-start(), calls=%async_computation.6 | async-start | bytes 3932160 | tf_op jit(solution)/shard_map/all_gather | solution.py:32
  209.5 296.7 %all-reduce.5.cloned.1.call-start = ((), (), s32[]{:S(2)}) async-start(), calls=%async_computation.7 | async-start | bytes 4194304 | tf_op jit(solution)/shard_map/psum | solution.py:34
  257.8 2.6 copy-start.2
  260.4 1.6 copy-start.1
  506.3 2.6 copy-start.3
Sparse Core Ops, SparseCore 0:
  8.9 66.1 all-gather.6
  76.7 62.0 all-gather.8
  140.4 62.0 all-gather.10
  207.7 50.0 all-reduce.2
  259.2 63.5 all-gather.12
  324.2 62.0 all-gather.14
  387.9 62.0 all-gather.16
  456.2 49.9 all-reduce.4
where the time goes:
time: 520 us
  waiting for transfers between devices  467 us (90%)
  matrix products  26.1 us (5%)
  between operations  13.6 us (3%)
  other arithmetic  11.6 us (2%)
    all_gather x2, waiting for transfers between devices, half_step(): lax.all_gather(up_w, 'fs', axis=0, tiled=True)  127 us
    all_gather x2, waiting for transfers between devices, half_step(): lax.all_gather(gate_w, 'fs', axis=0, tiled=True)  126 us
    all_gather x2, waiting for transfers between devices, half_step(): down_full = lax.all_gather(down_w, 'fs', axis=1, tiled=True)  112 us
    psum x2, waiting for transfers between devices, half_step(): lax.psum(partial_value, 'tp').astype(jnp.float32).astype(jnp.bfloat16)  98.1 us
    dot_general x2, matrix products, half_step(): both = jnp.dot(stream, joined, preferred_element_type=jnp.float32)  14.9 us
    dot_general x2, matrix products, rounded_term(): jnp.dot(stream_rows, down_full, preferred_element_type=jnp.float32)  11.2 us
  transfers between devices with their start and end apart: 8, of which 8 were waited for; matrix products, arithmetic and copies ran while one was open for 4% of the time, Pallas kernels for 0%

commit v1 on v0

--- a/solution.py
+++ b/solution.py
@@ -31,7 +31,11 @@
     scale = 2.0**0.25
     down_full = lax.all_gather(down_w, "fs", axis=1, tiled=True)
     partial_value = rounded_term(hidden, down_full)
-    branch = lax.psum(partial_value, "tp").astype(jnp.float32).astype(jnp.bfloat16)
+    branch = (
+        jnp.sum(lax.all_gather(partial_value, "tp"), axis=0)
+        .astype(jnp.float32)
+        .astype(jnp.bfloat16)
+    )
     return post_norm(
         scale * stream.astype(jnp.float32) + 0.5 * branch.astype(jnp.float32), gain, shift
     )

time: 520 us -> 541 us (1.040)
  other arithmetic: 11.6 us -> 27.1 us
  waiting for transfers between devices: 467 us -> 473 us
    all_gather x0 -> x2, waiting for transfers between devices: none -> 112 us  [half_step(): lax.all_gather(partial_value, 'tp')]
    psum x2 -> x0, waiting for transfers between devices: 98.1 us -> none  [half_step(): lax.psum(partial_value, 'tp').astype(jnp.float32).astype(jnp.bfloat16)]
    reduce_sum x0 -> x2, other arithmetic: none -> 13.1 us  [half_step(): jnp.sum(lax.all_gather(partial_value, 'tp'), axis=0).astype(jnp.float32)]
    all_gather x2, waiting for transfers between devices: 126 us -> 118 us  [half_step(): lax.all_gather(gate_w, 'fs', axis=0, tiled=True)]
  transfers between devices with their start and end apart: 8 -> 8, of which waited for: 8 -> 8; matrix products, arithmetic and copies ran while one was open for 4% -> 5% of each run, Pallas kernels for 0% -> 0%
where the time goes in v1:
time: 541 us
  waiting for transfers between devices  473 us (87%)
  other arithmetic  27.1 us (5%)
  matrix products  26.1 us (5%)
  between operations  13.6 us (3%)
    all_gather x2, waiting for transfers between devices, half_step(): lax.all_gather(up_w, 'fs', axis=0, tiled=True)  127 us
    all_gather x2, waiting for transfers between devices, half_step(): lax.all_gather(gate_w, 'fs', axis=0, tiled=True)  118 us
    all_gather x2, waiting for transfers between devices, half_step(): down_full = lax.all_gather(down_w, 'fs', axis=1, tiled=True)  112 us
    all_gather x2, waiting for transfers between devices, half_step(): lax.all_gather(partial_value, 'tp')  112 us
    dot_general x2, matrix products, half_step(): both = jnp.dot(stream, joined, preferred_element_type=jnp.float32)  14.9 us
    reduce_sum x2, other arithmetic, half_step(): jnp.sum(lax.all_gather(partial_value, 'tp'), axis=0).astype(jnp.float32)  13.1 us
    dot_general x2, matrix products, rounded_term(): jnp.dot(stream_rows, down_full, preferred_element_type=jnp.float32)  11.2 us
  transfers between devices with their start and end apart: 8, of which 8 were waited for; matrix products, arithmetic and copies ran while one was open for 5% of the time, Pallas kernels for 0%

profile of v1, /device:TPU:0, one launch (start us, length us, event | category | flops | bytes accessed | tf_op | source)
XLA Modules:
  0.0 540.7 jit_solution(26409251204660456)
XLA Ops:
  6.5 0.0 all-gather.11.cloned.1.call-start
  6.5 0.7 all-gather.11.cloned.1.call-update
  7.3 0.0 all-gather.13.cloned.1.call-start
  7.3 0.7 all-gather.13.cloned.1.call-update
  8.0 0.0 all-gather.15.cloned.1.call-start
  8.1 0.7 all-gather.15.cloned.1.call-update
  8.7 0.0 all-gather.23.cloned.1.call-start
  8.8 66.3 %all-gather.11.cloned.1.call-done = bf16[2048,768]{1,0:T(8,128)(2,1)} async-done(((bf16[512,768]{1,0:T(8,128)(2,1)}), bf16[2048,768]{1,0:T(8,128)(2,1)}) %all-gather.11.cloned.1.call-update) | async-done | bytes 3145744 | tf_op jit(solution)/shard_map/all_gather | solution.py:22
  75.1 63.7 %all-gather.13.cloned.1.call-done = bf16[2048,768]{1,0:T(8,128)(2,1)} async-done(((bf16[512,768]{1,0:T(8,128)(2,1)}), bf16[2048,768]{1,0:T(8,128)(2,1)}) %all-gather.13.cloned.1.call-update) | async-done | bytes 3145744 | tf_op jit(solution)/shard_map/all_gather | solution.py:23
  138.8 6.9 %fusion.8 = f32[512,1536]{0,1:T(8,128)S(1)} fusion(bf16[512,2048]{1,0:T(8,128)(2,1)} %param.9, bf16[2048,768]{1,0:T(8,128)(2,1)} %all-gather.13.cloned.1.call-done, bf16[2048,768]{1,0:T(8,128)(2,1)} %all-gather.11.cloned.1.call-done), kind=kOutput, calls=%fused_computation.14 | convolution fusion | flops 3233808384 | bytes 11534336 | tf_op jit(solution)/shard_map/dot_general | solution.py:27
  145.7 56.7 %all-gather.15.cloned.1.call-done = bf16[768,2048]{1,0:T(8,128)(2,1)} async-done(((bf16[768,512]{1,0:T(8,128)(2,1)}), bf16[768,2048]{1,0:T(8,128)(2,1)}) %all-gather.15.cloned.1.call-update) | async-done | bytes 3145744 | tf_op jit(solution)/shard_map/all_gather | solution.py:32
  202.5 5.1 convolution_convert_fusion.1
  207.6 0.0 copy-start.3
  207.6 0.0 copy-start.4
  207.6 0.0 all-gather.23.cloned.1.call-update
  207.6 0.0 all-gather.17.cloned.1.call-start
  207.7 0.5 all-gather.17.cloned.1.call-update
  208.2 0.0 all-gather.19.cloned.1.call-start
  208.3 0.5 all-gather.19.cloned.1.call-update
  208.8 0.0 all-gather.21.cloned.1.call-start
  208.8 0.7 all-gather.21.cloned.1.call-update
  209.5 0.2 all-gather.25.cloned.1.call-start
  209.8 0.0 copy-done.3
  209.8 0.0 copy-done.4
  209.8 54.8 %all-gather.23.cloned.1.call-done = bf16[2048,2048]{1,0:T(8,128)(2,1)} async-done(((bf16[512,2048]{1,0:T(8,128)(2,1)}), bf16[2048,2048]{1,0:T(8,128)(2,1)}) %all-gather.23.cloned.1.call-update) | async-done | bytes 8388624 | tf_op jit(solution)/shard_map/all_gather | solution.py:35
  264.7 5.7 %reduce_sum.60 = bf16[512,2048]{1,0:T(8,128)(2,1)S(1)} reduce(bf16[4,512,2048]{2,1,0:T(8,128)(2,1)} %bitcast.12, bf16[]{:T(256)} %constant.16.clone.1), dimensions={0}, to_apply=%region_0.1 | reduce | flops 3145728 | bytes 10485762 | tf_op jit(solution)/shard_map/reduce_sum | solution.py:35
  270.4 0.0 copy-start.1
  270.4 0.0 copy-start.2
  270.4 3.4 fusion.11
  273.8 0.0 copy-done.2
  273.8 1.2 multiply_reduce_fusion.1
  274.9 0.0 copy-done.1
  274.9 3.0 add_convert_fusion.1
  278.0 51.6 %all-gather.17.cloned.1.call-done = bf16[2048,768]{1,0:T(8,128)(2,1)} async-done(((bf16[512,768]{1,0:T(8,128)(2,1)}), bf16[2048,768]{1,0:T(8,128)(2,1)}) %all-gather.17.cloned.1.call-update) | async-done | bytes 3145744 | tf_op jit(solution)/shard_map/all_gather | solution.py:22
  329.6 63.5 %all-gather.19.cloned.1.call-done = bf16[2048,768]{1,0:T(8,128)(2,1)} async-done(((bf16[512,768]{1,0:T(8,128)(2,1)}), bf16[2048,768]{1,0:T(8,128)(2,1)}) %all-gather.19.cloned.1.call-update) | async-done | bytes 3145744 | tf_op jit(solution)/shard_map/all_gather | solution.py:23
  393.1 7.9 %fusion.4 = f32[512,1536]{0,1:T(8,128)} fusion(bf16[512,2048]{1,0:T(8,128)(2,1)S(1)} %add_convert_fusion.1, bf16[2048,768]{1,0:T(8,128)(2,1)} %all-gather.19.cloned.1.call-done, bf16[2048,768]{1,0:T(8,128)(2,1)} %all-gather.17.cloned.1.call-done), kind=kOutput, calls=%fused_computation.4 | convolution fusion | flops 3233808384 | bytes 11534336 | tf_op jit(solution)/shard_map/dot_general | solution.py:27
  401.1 55.7 %all-gather.21.cloned.1.call-done = bf16[768,2048]{1,0:T(8,128)(2,1)} async-done(((bf16[768,512]{1,0:T(8,128)(2,1)}), bf16[768,2048]{1,0:T(8,128)(2,1)}) %all-gather.21.cloned.1.call-update) | async-done | bytes 3145744 | tf_op jit(solution)/shard_map/all_gather | solution.py:32
  456.8 6.1 %convolution_convert_fusion = bf16[512,2048]{1,0:T(8,128)(2,1)} fusion(bf16[768,2048]{1,0:T(8,128)(2,1)} %all-gather.21.cloned.1.call-done, f32[512,1536]{0,1:T(8,128)} %fusion.4), kind=kOutput, calls=%fused_computation.15 | convolution fusion | flops 1614020608 | bytes 8388608 | tf_op jit(solution)/shard_map/dot_general | solution.py:15
  462.9 0.0 all-gather.25.cloned.1.call-update
  462.9 57.1 %all-gather.25.cloned.1.call-done = bf16[2048,2048]{1,0:T(8,128)(2,1)} async-done(((bf16[512,2048]{1,0:T(8,128)(2,1)}), bf16[2048,2048]{1,0:T(8,128)(2,1)}) %all-gather.25.cloned.1.call-update) | async-done | bytes 8388624 | tf_op jit(solution)/shard_map/all_gather | solution.py:35
  520.0 7.4 %reduce_sum.63 = bf16[512,2048]{1,0:T(8,128)(2,1)} reduce(bf16[4,512,2048]{2,1,0:T(8,128)(2,1)} %bitcast.13, bf16[]{:T(256)} %constant.16.clone.1), dimensions={0}, to_apply=%region_3.4 | reduce | flops 3145728 | bytes 10485762 | tf_op jit(solution)/shard_map/reduce_sum | solution.py:35
  527.4 0.0 copy-start
  527.4 2.6 fusion.12
  530.0 0.0 copy-done
  530.0 1.2 multiply_reduce_fusion
  531.2 2.6 add_convert_fusion
  (6 shorter events, 0.1 us)
Async XLA Ops:
  6.5 68.6 %all-gather.11.cloned.1.call-start = ((), (), s32[]{:S(2)}) async-start(), calls=%async_computation | async-start | bytes 3932160 | tf_op jit(solution)/shard_map/all_gather | solution.py:22
  7.3 131.5 %all-gather.13.cloned.1.call-start = ((), (), s32[]{:S(2)}) async-start(), calls=%async_computation.1 | async-start | bytes 3932160 | tf_op jit(solution)/shard_map/all_gather | solution.py:23
  8.0 194.5 %all-gather.15.cloned.1.call-start = ((), (), s32[]{:S(2)}) async-start(), calls=%async_computation.2 | async-start | bytes 3932160 | tf_op jit(solution)/shard_map/all_gather | solution.py:32
  8.7 255.9 %all-gather.23.cloned.1.call-start = ((), (), s32[]{:S(2)}) async-start(), calls=%async_computation.6 | async-start | bytes 10485760 | tf_op jit(solution)/shard_map/all_gather | solution.py:35
  207.6 2.2 copy-start.3
  207.6 2.2 copy-start.4
  207.6 122.0 %all-gather.17.cloned.1.call-start = ((), (), s32[]{:S(2)}) async-start(), calls=%async_computation.3 | async-start | bytes 3932160 | tf_op jit(solution)/shard_map/all_gather | solution.py:22
  208.2 184.9 %all-gather.19.cloned.1.call-start = ((), (), s32[]{:S(2)}) async-start(), calls=%async_computation.4 | async-start | bytes 3932160 | tf_op jit(solution)/shard_map/all_gather | solution.py:23
  208.8 248.0 %all-gather.21.cloned.1.call-start = ((), (), s32[]{:S(2)}) async-start(), calls=%async_computation.5 | async-start | bytes 3932160 | tf_op jit(solution)/shard_map/all_gather | solution.py:32
  209.5 310.4 %all-gather.25.cloned.1.call-start = ((), (), s32[]{:S(2)}) async-start(), calls=%async_computation.7 | async-start | bytes 10485760 | tf_op jit(solution)/shard_map/all_gather | solution.py:35
  270.4 4.6 copy-start.1
  270.4 3.4 copy-start.2
  527.4 2.6 copy-start
Sparse Core Ops, SparseCore 0:
  8.9 66.1 all-gather.10
  76.7 62.0 all-gather.12
  140.4 62.0 all-gather.14
  207.7 56.8 all-gather.22
  266.1 63.4 all-gather.16
  331.0 62.0 all-gather.18
  394.7 62.0 all-gather.20
  463.0 56.8 all-gather.24
